TPU v7x, 32 devices: a whole 2x2x4 slice. The times are simulated.
32 devices in a mesh: ep: 4 (over y, x), tp: 8 (over z, core).
Axes of the slice: x: 2, y: 2, z: 4, core: 2. Of those that a mesh axis runs over, the one named last changes fastest.
Arguments:
- residual: bfloat16 [128, 2048], P('ep'), may hold values from -20 to 20
- cache_latent: bfloat16 [128, 2048, 256], P(('ep', 'tp')), may hold values from -12 to 12
- cache_rope: bfloat16 [128, 32, 2048], P(('ep', 'tp')), may hold values from -6 to 6
- lengths: int32 [128], P(('ep', 'tp')), may hold values from 2 to 2048, as said below
- query_latent: bfloat16 [128, 32, 256], P(('ep', 'tp')), may hold values from -250 to 250
- query_rope: bfloat16 [128, 32, 32], P(('ep', 'tp')), may hold values from -6 to 6
- norm_gain: bfloat16 [2048], replicated, may hold values from 0.099609375 to 1.8984375
- latent_weight: bfloat16 [2048, 256], replicated, may hold values from -0.125 to 0.125
- latent_gain: bfloat16 [256], replicated, may hold values from 0.099609375 to 1.8984375
- rope_weight: bfloat16 [32, 2048], replicated, may hold values from -0.125 to 0.125
- value_weight: bfloat16 [256, 2048], replicated, may hold values from -0.375 to 0.375
- out_weight: bfloat16 [2048, 2048], P('tp'), may hold values from -1 to 1
- mixer_gain: bfloat16 [2048], replicated, may hold values from 0.099609375 to 1.8984375
- group_router: bfloat16 [2048, 4], replicated, may hold values from -0.0625 to 0.0625
- expert_router: bfloat16 [2048, 8], replicated, may hold values from -0.0625 to 0.0625
- expert_ids: int32 [128, 2], P('ep'), may hold values from 0 to 7, as said below
- gate_weight: bfloat16 [8, 2048, 4096], P('ep', None, 'tp'), may hold values from -0.125 to 0.125
- up_weight: bfloat16 [8, 2048, 4096], P('ep', None, 'tp'), may hold values from -0.125 to 0.125
- down_weight: bfloat16 [8, 4096, 2048], P('ep', 'tp'), may hold values from -0.75 to 0.75
Outputs:
- mixed: bfloat16 [128, 2048], P('ep')
- new_latent: bfloat16 [128, 256], P(('ep', 'tp'))
- new_rope_key: bfloat16 [128, 32], P(('ep', 'tp'))
Inputs may be any that keep to these rules, and one draw needn't show every extreme that they name: `lengths`: every sequence has 2 or more cached positions, and in every draw some sequence has all 2048. `expert_ids`: each row names 2 different experts of one group; group g holds experts g * 2 to g * 2 + 1. Among the rows of one index of ep (aligned blocks of 32 rows) no expert is named more than 16 times, and in every draw some expert is named exactly 16 times in every block.
All inputs are finite; a program needn't handle non-finite values.
Results may differ from a plain program's by a relative error of at most 0.012.
Values may be sent and summed in bfloat16 or wider, within the bound.
A program may use at most 64 MiB of HBM per device.

v0:
```python
import jax
import jax.numpy as jnp
from jax import lax
from jax.sharding import PartitionSpec as P

H = 32
KV = 256
ROPE = 32
NOPE = 64
V = 64
GROUPS = 4
TOPK = 2
NORM_EPSILON = 1e-06
ROPE_BASE = 10000.0


def inverse_rms(values):
    return lax.rsqrt(jnp.mean(values * values, axis=-1, keepdims=True) + NORM_EPSILON)


def rotate(vector, position):
    half_width = vector.shape[-1] // 2
    frequency = ROPE_BASE ** (
        -jnp.arange(0, vector.shape[-1], 2, dtype=jnp.float32) / vector.shape[-1]
    )
    angles = position[..., None] * frequency
    lower_half = vector[..., :half_width]
    upper_half = vector[..., half_width:]
    return jnp.concatenate(
        [
            lower_half * jnp.cos(angles) - upper_half * jnp.sin(angles),
            upper_half * jnp.cos(angles) + lower_half * jnp.sin(angles),
        ],
        axis=-1,
    )


def dispatch_table(expert_rows, experts, capacity):
    flat_ids = expert_rows.reshape(-1)
    hit_table = (flat_ids[:, None] == jnp.arange(experts, dtype=jnp.int32)[None, :]).astype(
        jnp.int32
    )
    slot_rank = jnp.sum((jnp.cumsum(hit_table, axis=0) - hit_table) * hit_table, axis=1)
    slot_index = flat_ids * capacity + slot_rank
    picked = (
        slot_index[None, :] == jnp.arange(experts * capacity, dtype=jnp.int32)[:, None]
    ).astype(jnp.float32)
    return picked.reshape(experts * capacity, expert_rows.shape[0], expert_rows.shape[1])


def route_weights(expert_in, group_router, expert_router, expert_ids, per_group):
    group_logits = jnp.dot(expert_in, group_router, preferred_element_type=jnp.float32)
    expert_logits = jnp.dot(expert_in, expert_router, preferred_element_type=jnp.float32)
    chosen = expert_ids[:, 0] // per_group
    group_hit = (
        jnp.arange(group_logits.shape[1], dtype=jnp.int32)[None, :] == chosen[:, None]
    ).astype(jnp.float32)
    chosen_logit = jnp.sum(group_logits * group_hit, axis=1, keepdims=True)
    group_share = 1.0 / jnp.sum(jnp.exp(group_logits - chosen_logit), axis=1)
    expert_hit = (
        expert_ids[:, :, None] == jnp.arange(expert_logits.shape[1], dtype=jnp.int32)[None, None, :]
    ).astype(jnp.float32)
    picked_logit = jnp.sum(expert_hit * expert_logits[:, None, :], axis=2)
    inner_share = 1.0 / jnp.sum(
        jnp.exp(picked_logit[:, None, :] - picked_logit[:, :, None]), axis=2
    )
    return group_share[:, None] * inner_share


def on_device(
    residual,
    cache_latent,
    cache_rope,
    lengths,
    query_latent,
    query_rope,
    norm_gain,
    latent_weight,
    latent_gain,
    rope_weight,
    value_weight,
    out_weight,
    mixer_gain,
    group_router,
    expert_router,
    expert_ids,
    gate_weight,
    up_weight,
    down_weight,
):
    ep_count = lax.axis_size("ep")
    seq_count = cache_latent.shape[0]
    group_rows = residual.shape[0]
    model_width = residual.shape[1]
    resid_f = residual.astype(jnp.float32)
    own_rows = lax.dynamic_slice_in_dim(resid_f, lax.axis_index("tp") * seq_count, seq_count, 0)
    normed = (own_rows * inverse_rms(own_rows) * norm_gain.astype(jnp.float32)).astype(jnp.bfloat16)
    latent_raw = jnp.dot(normed, latent_weight, preferred_element_type=jnp.float32)
    new_latent = (latent_raw * inverse_rms(latent_raw) * latent_gain.astype(jnp.float32)).astype(
        jnp.bfloat16
    )
    positions = lengths.astype(jnp.float32)
    rope_raw = jnp.dot(normed, rope_weight.T, preferred_element_type=jnp.float32)
    new_rope_key = rotate(rope_raw, positions).astype(jnp.bfloat16)
    query_turned = rotate(query_rope.astype(jnp.float32), positions[:, None]).astype(jnp.bfloat16)
    score_scale = (NOPE + ROPE) ** (-0.5)
    cached = (
        jnp.einsum("shc,spc->shp", query_latent, cache_latent, preferred_element_type=jnp.float32)
        + jnp.einsum("shr,srp->shp", query_turned, cache_rope, preferred_element_type=jnp.float32)
    ) * score_scale
    keeping = (
        jnp.arange(cache_latent.shape[1], dtype=jnp.int32)[None, None, :] < lengths[:, None, None]
    )
    cached = jnp.where(keeping, cached, -jnp.inf)
    fresh = (
        jnp.einsum("shc,sc->sh", query_latent, new_latent, preferred_element_type=jnp.float32)
        + jnp.einsum("shr,sr->sh", query_turned, new_rope_key, preferred_element_type=jnp.float32)
    ) * score_scale
    row_top = jnp.maximum(jnp.max(cached, axis=2), fresh)
    cached_exp = jnp.exp(cached - row_top[:, :, None])
    fresh_exp = jnp.exp(fresh - row_top)
    denominator = jnp.sum(cached_exp, axis=2) + fresh_exp
    cached_weight = (cached_exp / denominator[:, :, None]).astype(jnp.bfloat16)
    fresh_weight = (fresh_exp / denominator).astype(jnp.bfloat16)
    mixed_latent = (
        jnp.einsum("shp,spc->shc", cached_weight, cache_latent, preferred_element_type=jnp.float32)
        + fresh_weight.astype(jnp.float32)[:, :, None] * new_latent.astype(jnp.float32)[:, None, :]
    ).astype(jnp.bfloat16)
    head_values = jnp.einsum(
        "shc,chv->shv",
        mixed_latent,
        value_weight.reshape(KV, H, V),
        preferred_element_type=jnp.float32,
    ).astype(jnp.bfloat16)
    by_heads = lax.all_to_all(head_values, "tp", split_axis=1, concat_axis=0, tiled=True)
    head_terms = jnp.dot(
        by_heads.reshape(group_rows, -1), out_weight, preferred_element_type=jnp.float32
    )
    attended = lax.psum(head_terms, "tp")
    after_attention = (resid_f + attended).astype(jnp.bfloat16)
    after_f = after_attention.astype(jnp.float32)
    expert_in = (after_f * inverse_rms(after_f) * mixer_gain.astype(jnp.float32)).astype(
        jnp.bfloat16
    )
    experts = expert_router.shape[1]
    capacity = 2 * group_rows * TOPK // experts
    route_weight = route_weights(
        expert_in, group_router, expert_router, expert_ids, experts // GROUPS
    )
    picked = dispatch_table(expert_ids, experts, capacity)
    select_rows = jnp.sum(picked, axis=2).astype(jnp.bfloat16)
    outbound = jnp.dot(select_rows, expert_in, preferred_element_type=jnp.float32).astype(
        jnp.bfloat16
    )
    outbound = outbound.reshape(ep_count, gate_weight.shape[0], capacity, model_width)
    rows = lax.all_to_all(outbound, "ep", split_axis=0, concat_axis=0, tiled=True)
    gate_value = jnp.einsum("secd,edf->secf", rows, gate_weight, preferred_element_type=jnp.float32)
    up_value = jnp.einsum("secd,edf->secf", rows, up_weight, preferred_element_type=jnp.float32)
    activation = (jax.nn.silu(gate_value) * up_value).astype(jnp.bfloat16)
    expert_terms = jnp.einsum(
        "secf,efd->secd", activation, down_weight, preferred_element_type=jnp.float32
    )
    combine = jnp.sum(picked * route_weight[None, :, :], axis=2).T
    summed_terms = lax.psum_scatter(expert_terms, "tp", scatter_dimension=3, tiled=True)
    returned_terms = lax.all_to_all(summed_terms, "ep", split_axis=0, concat_axis=0, tiled=True)
    share_width = returned_terms.shape[3]
    moe_part = jnp.dot(
        combine, returned_terms.reshape(-1, share_width), precision=lax.Precision.HIGHEST
    )
    after_cols = lax.dynamic_slice_in_dim(
        after_f, lax.axis_index("tp") * share_width, share_width, 1
    )
    mixed_share = (after_cols + moe_part).astype(jnp.bfloat16)
    mixed = lax.all_gather(mixed_share, "tp", axis=1, tiled=True)
    return (mixed, new_latent, new_rope_key)


def solution(mesh):
    in_specs = (
        P("ep", None),
        P(("ep", "tp"), None, None),
        P(("ep", "tp"), None, None),
        P(("ep", "tp")),
        P(("ep", "tp"), None, None),
        P(("ep", "tp"), None, None),
        P(),
        P(),
        P(),
        P(),
        P(),
        P("tp", None),
        P(),
        P(),
        P(),
        P("ep", None),
        P("ep", None, "tp"),
        P("ep", None, "tp"),
        P("ep", "tp", None),
    )
    out_specs = (P("ep", None), P(("ep", "tp"), None), P(("ep", "tp"), None))
    return jax.shard_map(
        on_device, mesh=mesh, in_specs=in_specs, out_specs=out_specs, check_vma=False
    )
```

profile of v0, /device:TPU:0, one launch (start us, length us, event | category | flops | bytes accessed | tf_op | source)
XLA Modules:
  0.0 177.1 jit_solution(6395437696958432695)
XLA Ops:
  7.2 0.8 convert_element_type.79
  8.0 0.7 iota_compare_fusion.2
  8.7 0.9 convert_element_type.77
  9.8 0.7 convert_element_type.80
  10.5 0.8 convert_element_type.78
  11.3 1.1 fusion.50
  12.4 1.6 multiply_reduce_fusion.2
  14.0 0.7 convert_element_type.82
  14.7 3.5 %fusion.58 = f32[4,32,2048]{2,1,0:T(8,128)S(1)} fusion(bf16[4,32,256]{2,1,0:T(8,128)(2,1)} %param.23, bf16[4,2048,256]{2,1,0:T(8,128)(2,1)} %param.20), kind=kOutput, calls=%fused_computation.90 | convolution fusion | flops 134217728 | bytes 5308416 | tf_op jit(solution)/shard_map/shc,spc->shp/dot_general | solution.py:108
  18.7 0.2 fusion.39
  18.9 0.5 fusion.54
  19.4 0.3 fusion.26
  19.8 1.5 copy.61
  21.3 3.1 %fusion.23 = bf16[4,32,256]{2,1,0:T(8,128)(2,1)S(1)} fusion(bf16[4,2048,256]{2,1,0:T(8,128)(2,1)} %param.20, f32[4,32,2048]{2,1,0:T(8,128)S(1)} %get-tuple-element.18, f32[4,32]{1,0:T(4,128)S(1)} %get-tuple-element.12, f32[4,32]{1,0:T(4,128)S(1)} %fusion.44, f32[4,256]{1,0:T(4,128)S(1)} %get-tuple-element.7, f32[4,32]{1,0:T(4,128)S(1)} %get-tuple-element.11), kind=kOutput, calls=%fused_computation.16 | convolution fusion | flops 135102464 | bytes 5314048 | tf_op jit(solution)/shard_map/shp,spc->shc/dot_general | solution.py:126
  24.4 0.4 fusion.55
  24.8 0.7 reshape.194
  25.5 6.4 %all-to-all-start = ((bf16[8,2,512]{2,1,0:T(2,128)(2,1)}), bf16[8,2,512]{2,1,0:T(2,128)(2,1)S(1)}, u32[]{:S(2)}, u32[]{:S(2)}) async-start(bf16[8,2,512]{2,1,0:T(2,128)(2,1)} %reshape.194), calls=%async_computation | async-start | bytes 32768 | tf_op jit(solution)/shard_map/all_to_all | solution.py:135
  32.7 4.8 %all-to-all-done = bf16[8,2,512]{2,1,0:T(2,128)(2,1)S(1)} async-done(((bf16[8,2,512]{2,1,0:T(2,128)(2,1)}), bf16[8,2,512]{2,1,0:T(2,128)(2,1)S(1)}, u32[]{:S(2)}, u32[]{:S(2)}) %all-to-all-start) | async-done | bytes 16416 | tf_op jit(solution)/shard_map/all_to_all | solution.py:135
  37.7 1.0 fusion.59
  38.8 53.8 %all-reduce.2.cloned.1.call-done = f32[32,2048]{1,0:T(8,128)} async-done(((f32[32,2048]{1,0:T(8,128)}), f32[32,2048]{1,0:T(8,128)}) %all-reduce.2.cloned.1.call-update) | async-done | bytes 262160 | tf_op jit(solution)/shard_map/psum | solution.py:139
  92.6 1.1 multiply_reduce_fusion
  94.3 0.3 convolution_convert_fusion
  94.6 10.6 %all_to_all.25 = bf16[4,2,16,2048]{3,2,1,0:T(8,128)(2,1)S(1)} all-to-all(bf16[4,2,16,2048]{3,2,1,0:T(8,128)(2,1)S(1)} %bitcast.81), channel_id=1, replica_groups=mesh['ep'=4,'tp'=8] {'ep'}, dimensions={0} | all-to-all | bytes 1048576 | tf_op jit(solution)/shard_map/all_to_all | solution.py:156
  105.2 3.0 %fusion.11 = f32[4,2,16,512]{3,2,0,1:T(8,128)S(1)} fusion(bf16[2,2048,512]{2,1,0:T(8,128)(2,1)} %param.35, bf16[4,2,16,2048]{3,2,1,0:T(8,128)(2,1)S(1)} %all_to_all.25), kind=kOutput, calls=%fused_computation.11 | convolution fusion | flops 268435456 | bytes 4980736 | tf_op jit(solution)/shard_map/secd,edf->secf/dot_general | solution.py:157
  108.2 6.0 %fusion.6 = f32[4,2,16,2048]{3,2,0,1:T(8,128)} fusion(bf16[2,512,2048]{2,1,0:T(8,128)(2,1)} %param.37, bf16[2,2048,512]{2,1,0:T(8,128)(2,1)} %param.36, bf16[4,2,16,2048]{3,2,1,0:T(8,128)(2,1)S(1)} %all_to_all.25, f32[4,2,16,512]{3,2,0,1:T(8,128)S(1)} %fusion.11), kind=kOutput, calls=%fused_computation.6 | convolution fusion | flops 537264128 | bytes 10223616 | tf_op jit(solution)/shard_map/secf,efd->secd/dot_general | solution.py:160
  114.3 30.9 %reduce-scatter.2.cloned.1.call-done = f32[4,2,16,256]{3,2,0,1:T(8,128)} async-done(((f32[4,2,16,2048]{3,2,0,1:T(8,128)}), f32[4,2,16,256]{3,2,0,1:T(8,128)}) %reduce-scatter.2.cloned.1.call-update) | async-done | bytes 131088 | tf_op jit(solution)/shard_map/reduce_scatter | solution.py:164
  145.2 1.6 copy.68
  146.8 3.7 %all-to-all-start.2 = ((f32[4,2,16,256]{3,2,1,0:T(8,128)}), f32[4,2,16,256]{3,2,1,0:T(8,128)S(1)}, u32[]{:S(2)}, u32[]{:S(2)}) async-start(f32[4,2,16,256]{3,2,1,0:T(8,128)} %copy.68), calls=%async_computation.3 | async-start | bytes 262144 | tf_op jit(solution)/shard_map/all_to_all | solution.py:165
  150.4 0.6 pad_maximum_fusion.3
  151.1 4.4 %all-to-all-done.2 = f32[4,2,16,256]{3,2,1,0:T(8,128)S(1)} async-done(((f32[4,2,16,256]{3,2,1,0:T(8,128)}), f32[4,2,16,256]{3,2,1,0:T(8,128)S(1)}, u32[]{:S(2)}, u32[]{:S(2)}) %all-to-all-start.2) | async-done | bytes 131104 | tf_op jit(solution)/shard_map/all_to_all | solution.py:165
  155.6 14.0 %all_gather.3 = bf16[32,2048]{1,0:T(8,128)(2,1)S(1)} all-gather(bf16[32,256]{1,0:T(8,128)(2,1)S(1)} %fusion.25), channel_id=1, replica_groups=mesh['ep'=4,'tp'=8] {'tp'}, dimensions={1}, use_global_device_ids=true | all-gather | bytes 147456 | tf_op jit(solution)/shard_map/all_gather | solution.py:174
  169.6 0.7 copy.94
  (57 shorter events, 2.6 us)
Async XLA Ops:
  7.2 30.6 %copy-start = (bf16[256,2048]{1,0:T(8,128)(2,1)S(1)}, bf16[256,2048]{1,0:T(8,128)(2,1)}, u32[]{:S(2)}) copy-start(bf16[256,2048]{1,0:T(8,128)(2,1)} %param.30) | copy-start | bytes 3145732
  7.2 11.1 %copy-start.3 = (bf16[4,32,256]{2,1,0:T(8,128)(2,1)S(1)}, bf16[4,32,256]{2,1,0:T(8,128)(2,1)}, u32[]{:S(2)}) copy-start(bf16[4,32,256]{2,1,0:T(8,128)(2,1)} %param.23) | copy-start | bytes 196612
  7.2 11.7 %copy-start.2 = (bf16[4,32,2048]{2,1,0:T(8,128)(2,1)S(1)}, bf16[4,32,2048]{2,1,0:T(8,128)(2,1)}, u32[]{:S(2)}) copy-start(bf16[4,32,2048]{2,1,0:T(8,128)(2,1)} %param.21) | copy-start | bytes 1572868
  18.3 6.1 %copy-start.7 = (bf16[4,256]{1,0:T(4,128)(2,1)}, bf16[4,256]{1,0:T(4,128)(2,1)S(1)}, u32[]{:S(2)}) copy-start(bf16[4,256]{1,0:T(4,128)(2,1)S(1)} %get-tuple-element.27) | copy-start | bytes 6148
  21.2 10.7 %copy-start.5 = (s32[32,2]{0,1:T(2,128)S(1)}, s32[32,2]{0,1:T(2,128)}, u32[]{:S(2)}) copy-start(s32[32,2]{0,1:T(2,128)} %param.34) | copy-start | bytes 772
  21.3 11.4 %copy-start.6 = (bf16[2048]{0:T(1024)(128)(2,1)S(1)}, bf16[2048]{0:T(1024)(128)(2,1)}, u32[]{:S(2)}) copy-start(bf16[2048]{0:T(1024)(128)(2,1)} %param.31) | copy-start | bytes 12292
  21.3 71.3 %copy-start.1 = (bf16[32,2048]{1,0:T(8,128)(2,1)S(1)}, bf16[32,2048]{1,0:T(8,128)(2,1)}, u32[]{:S(2)}) copy-start(bf16[32,2048]{1,0:T(8,128)(2,1)} %param.19) | copy-start | bytes 393220
  21.3 72.5 %copy-start.8 = (bf16[2048,4]{0,1:T(4,128)(2,1)S(1)}, bf16[2048,4]{0,1:T(4,128)(2,1)}, u32[]{:S(2)}) copy-start(bf16[2048,4]{0,1:T(4,128)(2,1)} %param.32) | copy-start | bytes 49156
  21.3 72.7 %copy-start.4 = (bf16[2048,8]{0,1:T(8,128)(2,1)S(1)}, bf16[2048,8]{0,1:T(8,128)(2,1)}, u32[]{:S(2)}) copy-start(bf16[2048,8]{0,1:T(8,128)(2,1)} %param.33) | copy-start | bytes 98308
  25.5 12.0 %all-to-all-start = ((bf16[8,2,512]{2,1,0:T(2,128)(2,1)}), bf16[8,2,512]{2,1,0:T(2,128)(2,1)S(1)}, u32[]{:S(2)}, u32[]{:S(2)}) async-start(bf16[8,2,512]{2,1,0:T(2,128)(2,1)} %reshape.194), calls=%async_computation | async-start | bytes 32768 | tf_op jit(solution)/shard_map/all_to_all | solution.py:135
  31.9 60.7 %all-reduce.2.cloned.1.call-start = ((), (), s32[]{:S(2)}) async-start(), calls=%async_computation.4 | async-start | bytes 524288 | tf_op jit(solution)/shard_map/psum | solution.py:139
  38.7 106.5 %reduce-scatter.2.cloned.1.call-start = ((), (), s32[]{:S(2)}) async-start(), calls=%async_computation.5 | async-start | bytes 1179648 | tf_op jit(solution)/shard_map/reduce_scatter | solution.py:164
  146.8 8.7 %all-to-all-start.2 = ((f32[4,2,16,256]{3,2,1,0:T(8,128)}), f32[4,2,16,256]{3,2,1,0:T(8,128)S(1)}, u32[]{:S(2)}, u32[]{:S(2)}) async-start(f32[4,2,16,256]{3,2,1,0:T(8,128)} %copy.68), calls=%async_computation.3 | async-start | bytes 262144 | tf_op jit(solution)/shard_map/all_to_all | solution.py:165
Sparse Core Ops, SparseCore 0:
  38.9 53.6 all-reduce.1
  114.4 30.7 reduce-scatter.1
where the time goes:
time: 178 us; the launch traced here: 177 us
  waiting for transfers between devices  93.9 us (53%)
  blocking collectives  24.5 us (14%)
  matrix products  21.4 us (12%)
  between operations  14.3 us (8%)
  starting transfers between devices  10.1 us (6%)
  other arithmetic  7.81 us (4%)
  local copies, waits for them, and re-layouts  5.06 us (3%)
    psum x1, waiting for transfers between devices, on_device(): attended = lax.psum(head_terms, 'tp')  53.8 us
    reduce_scatter x1, waiting for transfers between devices, on_device(): lax.psum_scatter(expert_terms, 'tp', scatter_dimension=3, tiled=True)  30.9 us
    all_gather x1, blocking collectives, on_device(): mixed = lax.all_gather(mixed_share, 'tp', axis=1, tiled=True)  14 us
    all_to_all x1, blocking collectives, on_device(): lax.all_to_all(outbound, 'ep', split_axis=0, concat_axis=0, tiled=True)  10.6 us
    all_to_all x1, starting transfers between devices, on_device(): lax.all_to_all(head_values, 'tp', split_axis=1, concat_axis=0, tiled=True)  6.35 us
    dot_general x1, matrix products, on_device(): jnp.einsum('secf,efd->secd', activation, down_weight, preferred_element_t...  6.04 us
    all_to_all x1, waiting for transfers between devices, on_device(): lax.all_to_all(head_values, 'tp', split_axis=1, concat_axis=0, tiled=True)  4.83 us
    all_to_all x1, waiting for transfers between devices, on_device(): lax.all_to_all(summed_terms, 'ep', split_axis=0, concat_axis=0, tiled=True)  4.38 us
  transfers between devices with their start and end apart: 4, of which 4 were waited for; matrix products, arithmetic and copies ran while one was open for 1% of the time, Pallas kernels for 0%

commit v1 on v0

--- a/solution.py
+++ b/solution.py
@@ -136,7 +136,8 @@
     head_terms = jnp.dot(
         by_heads.reshape(group_rows, -1), out_weight, preferred_element_type=jnp.float32
     )
-    attended = lax.psum(head_terms, "tp")
+    pieces = lax.all_gather(head_terms, "tp")
+    attended = jnp.sum(pieces, axis=0)
     after_attention = (resid_f + attended).astype(jnp.bfloat16)
     after_f = after_attention.astype(jnp.float32)
     expert_in = (after_f * inverse_rms(after_f) * mixer_gain.astype(jnp.float32)).astype(

time: 178 us -> 153 us (0.86)
  waiting for transfers between devices: 93.9 us -> 61.8 us
  blocking collectives: 24.5 us -> 38.1 us
  starting transfers between devices: 10.1 us -> 3.69 us
    psum x1 -> x0, waiting for transfers between devices: 53.8 us -> none  [on_device(): attended = lax.psum(head_terms, 'tp')]
    all_gather x0 -> x1, waiting for transfers between devices: none -> 26.7 us  [on_device(): pieces = lax.all_gather(head_terms, 'tp')]
    all_to_all x0 -> x1, blocking collectives: none -> 11.8 us  [on_device(): lax.all_to_all(head_values, 'tp', split_axis=1, concat_axis=0, tiled=True)]
    all_to_all x1 -> x0, starting transfers between devices: 6.35 us -> none  [on_device(): lax.all_to_all(head_values, 'tp', split_axis=1, concat_axis=0, tiled=True)]
    all_to_all x1 -> x0, waiting for transfers between devices: 4.83 us -> none  [on_device(): lax.all_to_all(head_values, 'tp', split_axis=1, concat_axis=0, tiled=True)]
    all_to_all x1, blocking collectives: 10.6 us -> 12.4 us  [on_device(): lax.all_to_all(outbound, 'ep', split_axis=0, concat_axis=0, tiled=True)]
  transfers between devices with their start and end apart: 4 -> 3, of which waited for: 4 -> 3; matrix products, arithmetic and copies ran while one was open for 1% -> 1% of each run, Pallas kernels for 0% -> 0%
where the time goes in v1:
time: 153 us; the launch traced here: 152 us
  waiting for transfers between devices  61.8 us (40%)
  blocking collectives  38.1 us (25%)
  matrix products  21.3 us (14%)
  between operations  14.4 us (9%)
  other arithmetic  8.57 us (6%)
  local copies, waits for them, and re-layouts  4.45 us (3%)
  starting transfers between devices  3.69 us (2%)
    reduce_scatter x1, waiting for transfers between devices, on_device(): lax.psum_scatter(expert_terms, 'tp', scatter_dimension=3, tiled=True)  30.7 us
    all_gather x1, waiting for transfers between devices, on_device(): pieces = lax.all_gather(head_terms, 'tp')  26.7 us
    all_gather x1, blocking collectives, on_device(): mixed = lax.all_gather(mixed_share, 'tp', axis=1, tiled=True)  14 us
    all_to_all x1, blocking collectives, on_device(): lax.all_to_all(outbound, 'ep', split_axis=0, concat_axis=0, tiled=True)  12.4 us
    all_to_all x1, blocking collectives, on_device(): lax.all_to_all(head_values, 'tp', split_axis=1, concat_axis=0, tiled=True)  11.8 us
    dot_general x1, matrix products, on_device(): jnp.einsum('secf,efd->secd', activation, down_weight, preferred_element_t...  6.04 us
    all_to_all x1, waiting for transfers between devices, on_device(): lax.all_to_all(summed_terms, 'ep', split_axis=0, concat_axis=0, tiled=True)  4.38 us
    all_to_all x1, starting transfers between devices, on_device(): lax.all_to_all(summed_terms, 'ep', split_axis=0, concat_axis=0, tiled=True)  3.61 us
  transfers between devices with their start and end apart: 3, of which 3 were waited for; matrix products, arithmetic and copies ran while one was open for 1% of the time, Pallas kernels for 0%

profile of v1, /device:TPU:0, one launch (start us, length us, event | category | flops | bytes accessed | tf_op | source)
XLA Modules:
  0.0 152.4 jit_solution(17331043599545432066)
XLA Ops:
  7.3 0.8 convert_element_type.79
  8.0 0.7 iota_compare_fusion.2
  8.8 0.9 convert_element_type.77
  9.8 0.7 convert_element_type.80
  10.5 0.8 convert_element_type.78
  11.3 1.1 fusion.50
  12.4 1.6 %multiply_reduce_fusion.2 = (f32[4]{0:T(128)S(1)}, f32[4,256]{1,0:T(4,128)S(1)}) fusion(bf16[2048,256]{1,0:T(8,128)(2,1)} %param.26, f32[32,2048]{1,0:T(8,128)S(1)} %convert_element_type.77, s32[]{:T(128)S(6)} %select_n.17, f32[2048]{0:T(1024)S(1)} %convert_element_type.80, f32[4]{0:T(128)S(1)} %add_rsqrt_fusion.2), kind=kOutput, calls=%fused_computation.53 | convolution fusion | flops 4220924 | bytes 1094164 | tf_op jit(solution)/shard_map/dot_general | solution.py:98
  14.1 0.7 convert_element_type.82
  14.7 3.5 %fusion.58 = f32[4,32,2048]{2,1,0:T(8,128)S(1)} fusion(bf16[4,32,256]{2,1,0:T(8,128)(2,1)} %param.23, bf16[4,2048,256]{2,1,0:T(8,128)(2,1)} %param.20), kind=kOutput, calls=%fused_computation.90 | convolution fusion | flops 134217728 | bytes 5308416 | tf_op jit(solution)/shard_map/shc,spc->shp/dot_general | solution.py:108
  18.8 0.2 fusion.39
  19.0 0.5 fusion.54
  19.5 0.3 fusion.26
  19.8 1.5 copy.61
  21.3 3.0 %fusion.23 = bf16[4,32,256]{2,1,0:T(8,128)(2,1)S(1)} fusion(bf16[4,2048,256]{2,1,0:T(8,128)(2,1)} %param.20, f32[4,32,2048]{2,1,0:T(8,128)S(1)} %get-tuple-element.18, f32[4,32]{1,0:T(4,128)S(1)} %get-tuple-element.12, f32[4,32]{1,0:T(4,128)S(1)} %fusion.44, f32[4,256]{1,0:T(4,128)S(1)} %get-tuple-element.7, f32[4,32]{1,0:T(4,128)S(1)} %get-tuple-element.11), kind=kOutput, calls=%fused_computation.16 | convolution fusion | flops 135102464 | bytes 5314048 | tf_op jit(solution)/shard_map/shp,spc->shc/dot_general | solution.py:126
  24.4 0.4 fusion.55
  24.9 11.8 %all_to_all.25 = bf16[8,2,512]{2,1,0:T(2,128)(2,1)S(1)} all-to-all(bf16[8,2,512]{2,1,0:T(2,128)(2,1)S(1)} %reshape.195), channel_id=1, replica_groups=mesh['ep'=4,'tp'=8] {'tp'}, dimensions={0} | all-to-all | bytes 32768 | tf_op jit(solution)/shard_map/all_to_all | solution.py:135
  36.9 1.0 fusion.59
  38.4 0.2 select_reduce_fusion.1
  38.8 26.7 %all-gather.3.cloned.1.call-done = f32[256,2048]{1,0:T(8,128)} async-done(((f32[32,2048]{1,0:T(8,128)}), f32[256,2048]{1,0:T(8,128)}) %all-gather.3.cloned.1.call-update) | async-done | bytes 2097168 | tf_op jit(solution)/shard_map/all_gather | solution.py:139
  65.5 1.7 %reduce_sum.113 = f32[32,2048]{1,0:T(8,128)S(1)} reduce(f32[8,32,2048]{2,1,0:T(8,128)} %bitcast.82, f32[]{:T(128)} %constant.56.clone.1), dimensions={0}, to_apply=%region_4.5 | reduce | flops 458752 | bytes 2359300 | tf_op jit(solution)/shard_map/reduce_sum | solution.py:140
  68.0 0.3 convolution_convert_fusion
  68.4 12.4 %all_to_all.26 = bf16[4,2,16,2048]{3,2,1,0:T(8,128)(2,1)S(1)} all-to-all(bf16[4,2,16,2048]{3,2,1,0:T(8,128)(2,1)S(1)} %bitcast.83), channel_id=1, replica_groups=mesh['ep'=4,'tp'=8] {'ep'}, dimensions={0} | all-to-all | bytes 1048576 | tf_op jit(solution)/shard_map/all_to_all | solution.py:157
  80.7 3.0 %fusion.11 = f32[4,2,16,512]{3,2,0,1:T(8,128)S(1)} fusion(bf16[2,2048,512]{2,1,0:T(8,128)(2,1)} %param.35, bf16[4,2,16,2048]{3,2,1,0:T(8,128)(2,1)S(1)} %all_to_all.26), kind=kOutput, calls=%fused_computation.11 | convolution fusion | flops 268435456 | bytes 4980736 | tf_op jit(solution)/shard_map/secd,edf->secf/dot_general | solution.py:158
  83.7 6.0 %fusion.6 = f32[4,2,16,2048]{3,2,0,1:T(8,128)} fusion(bf16[2,512,2048]{2,1,0:T(8,128)(2,1)} %param.37, bf16[2,2048,512]{2,1,0:T(8,128)(2,1)} %param.36, bf16[4,2,16,2048]{3,2,1,0:T(8,128)(2,1)S(1)} %all_to_all.26, f32[4,2,16,512]{3,2,0,1:T(8,128)S(1)} %fusion.11), kind=kOutput, calls=%fused_computation.6 | convolution fusion | flops 537264128 | bytes 10223616 | tf_op jit(solution)/shard_map/secf,efd->secd/dot_general | solution.py:161
  89.8 30.7 %reduce-scatter.2.cloned.1.call-done = f32[4,2,16,256]{3,2,0,1:T(8,128)} async-done(((f32[4,2,16,2048]{3,2,0,1:T(8,128)}), f32[4,2,16,256]{3,2,0,1:T(8,128)}) %reduce-scatter.2.cloned.1.call-update) | async-done | bytes 131088 | tf_op jit(solution)/shard_map/reduce_scatter | solution.py:165
  120.5 1.6 %copy.68 = f32[4,2,16,256]{3,2,1,0:T(8,128)} copy(f32[4,2,16,256]{3,2,0,1:T(8,128)} %reduce-scatter.2.cloned.1.call-done) | data formatting | bytes 262144 | tf_op jit(solution)/shard_map/reduce_scatter | solution.py:165
  122.1 3.6 %all-to-all-start.2 = ((f32[4,2,16,256]{3,2,1,0:T(8,128)}), f32[4,2,16,256]{3,2,1,0:T(8,128)S(1)}, u32[]{:S(2)}, u32[]{:S(2)}) async-start(f32[4,2,16,256]{3,2,1,0:T(8,128)} %copy.68), calls=%async_computation.3 | async-start | bytes 262144 | tf_op jit(solution)/shard_map/all_to_all | solution.py:166
  125.7 0.6 pad_maximum_fusion.3
  126.3 4.4 %all-to-all-done.2 = f32[4,2,16,256]{3,2,1,0:T(8,128)S(1)} async-done(((f32[4,2,16,256]{3,2,1,0:T(8,128)}), f32[4,2,16,256]{3,2,1,0:T(8,128)S(1)}, u32[]{:S(2)}, u32[]{:S(2)}) %all-to-all-start.2) | async-done | bytes 131104 | tf_op jit(solution)/shard_map/all_to_all | solution.py:166
  130.7 0.2 fusion.25
  130.9 14.0 %all_gather.11 = bf16[32,2048]{1,0:T(8,128)(2,1)S(1)} all-gather(bf16[32,256]{1,0:T(8,128)(2,1)S(1)} %fusion.25), channel_id=1, replica_groups=mesh['ep'=4,'tp'=8] {'tp'}, dimensions={1}, use_global_device_ids=true | all-gather | bytes 147456 | tf_op jit(solution)/shard_map/all_gather | solution.py:175
  144.9 0.7 copy.93
  (57 shorter events, 2.5 us)
Async XLA Ops:
  7.2 29.7 %copy-start = (bf16[256,2048]{1,0:T(8,128)(2,1)S(1)}, bf16[256,2048]{1,0:T(8,128)(2,1)}, u32[]{:S(2)}) copy-start(bf16[256,2048]{1,0:T(8,128)(2,1)} %param.30) | copy-start | bytes 3145732
  7.2 11.2 %copy-start.3 = (bf16[4,32,256]{2,1,0:T(8,128)(2,1)S(1)}, bf16[4,32,256]{2,1,0:T(8,128)(2,1)}, u32[]{:S(2)}) copy-start(bf16[4,32,256]{2,1,0:T(8,128)(2,1)} %param.23) | copy-start | bytes 196612
  7.2 11.8 %copy-start.2 = (bf16[4,32,2048]{2,1,0:T(8,128)(2,1)S(1)}, bf16[4,32,2048]{2,1,0:T(8,128)(2,1)}, u32[]{:S(2)}) copy-start(bf16[4,32,2048]{2,1,0:T(8,128)(2,1)} %param.21) | copy-start | bytes 1572868
  7.2 58.3 %all-gather.3.cloned.1.call-start = ((), (), s32[]{:S(2)}) async-start(), calls=%async_computation.5 | async-start | bytes 2359296 | tf_op jit(solution)/shard_map/all_gather | solution.py:139
  18.3 6.0 %copy-start.7 = (bf16[4,256]{1,0:T(4,128)(2,1)}, bf16[4,256]{1,0:T(4,128)(2,1)S(1)}, u32[]{:S(2)}) copy-start(bf16[4,256]{1,0:T(4,128)(2,1)S(1)} %get-tuple-element.27) | copy-start | bytes 6148
  21.3 16.7 %copy-start.6 = (bf16[2048]{0:T(1024)(128)(2,1)S(1)}, bf16[2048]{0:T(1024)(128)(2,1)}, u32[]{:S(2)}) copy-start(bf16[2048]{0:T(1024)(128)(2,1)} %param.31) | copy-start | bytes 12292
  21.3 16.7 %copy-start.5 = (s32[32,2]{0,1:T(2,128)S(1)}, s32[32,2]{0,1:T(2,128)}, u32[]{:S(2)}) copy-start(s32[32,2]{0,1:T(2,128)} %param.34) | copy-start | bytes 772
  24.4 42.9 %copy-start.1 = (bf16[32,2048]{1,0:T(8,128)(2,1)S(1)}, bf16[32,2048]{1,0:T(8,128)(2,1)}, u32[]{:S(2)}) copy-start(bf16[32,2048]{1,0:T(8,128)(2,1)} %param.19) | copy-start | bytes 393220
  24.4 43.1 %copy-start.8 = (bf16[2048,4]{0,1:T(4,128)(2,1)S(1)}, bf16[2048,4]{0,1:T(4,128)(2,1)}, u32[]{:S(2)}) copy-start(bf16[2048,4]{0,1:T(4,128)(2,1)} %param.32) | copy-start | bytes 49156
  24.4 43.3 %copy-start.4 = (bf16[2048,8]{0,1:T(8,128)(2,1)S(1)}, bf16[2048,8]{0,1:T(8,128)(2,1)}, u32[]{:S(2)}) copy-start(bf16[2048,8]{0,1:T(8,128)(2,1)} %param.33) | copy-start | bytes 98308
  37.9 82.6 %reduce-scatter.2.cloned.1.call-start = ((), (), s32[]{:S(2)}) async-start(), calls=%async_computation.4 | async-start | bytes 1179648 | tf_op jit(solution)/shard_map/reduce_scatter | solution.py:165
  122.1 8.6 %all-to-all-start.2 = ((f32[4,2,16,256]{3,2,1,0:T(8,128)}), f32[4,2,16,256]{3,2,1,0:T(8,128)S(1)}, u32[]{:S(2)}, u32[]{:S(2)}) async-start(f32[4,2,16,256]{3,2,1,0:T(8,128)} %copy.68), calls=%async_computation.3 | async-start | bytes 262144 | tf_op jit(solution)/shard_map/all_to_all | solution.py:166
Sparse Core Ops, SparseCore 0:
  38.1 27.3 all-gather.2
  89.9 30.5 reduce-scatter.1
